TPU v7x, 32 devices: a whole 2x2x4 slice. The times are simulated.
32 devices in a mesh: grp: 2 (over y), dp: 2 (over x), kv: 4 (over z), tp: 2 (over core).
Axes of the slice: x: 2, y: 2, z: 4, core: 2. Of those that a mesh axis runs over, the one named last changes fastest.
Arguments:
- tokens: bfloat16 [256, 4, 4096], P(('grp', 'dp'), None, ('kv', 'tp')), parts along dimension 0, may hold values from -160 to 160
- norm_gain: float32 [4096], replicated, may hold values from 0.1 to 1.9
- w_query: bfloat16 [4096, 16, 64], P(None, 'kv'), may hold values from -0.09375 to 0.09375
- w_key: bfloat16 [4096, 16, 64], P(None, 'kv'), may hold values from -0.09375 to 0.09375
- w_value: bfloat16 [4096, 16, 128], P(None, 'kv', 'tp'), may hold values from -0.09375 to 0.09375
- w_outgate: bfloat16 [4096, 16, 128], P(None, 'kv', 'tp'), may hold values from -0.09375 to 0.09375
- w_input: bfloat16 [4096, 16], replicated, may hold values from -0.09375 to 0.09375
- w_forget: bfloat16 [4096, 16], replicated, may hold values from -0.09375 to 0.09375
- forget_bias: float32 [16], replicated, may hold values from -1 to 4
- head_gain: float32 [16, 128], replicated, may hold values from 0.1 to 1.9
- w_out: bfloat16 [16, 128, 4096], P('kv', 'tp'), may hold values from -0.125 to 0.125
- memory: float32 [256, 16, 128, 64], P(('grp', 'dp'), 'kv', 'tp'), parts along dimension 0, may hold values from -12 to 12
- normalizer: float32 [256, 16, 64], P(('grp', 'dp'), 'kv'), parts along dimension 0, may hold values from -12 to 12
- stabilizer: float32 [256, 16], P(('grp', 'dp'), 'kv'), parts along dimension 0, may hold values from -1 to 1
- prev_keys: bfloat16 [256, 4, 16, 64], P(('grp', 'dp'), None, 'kv'), parts along dimension 0, may hold values from -6 to 6
- prev_values: bfloat16 [256, 4, 16, 128], P(('grp', 'dp'), None, 'kv', 'tp'), parts along dimension 0, may hold values from -6 to 6
- prev_input: float32 [256, 4, 16], P(('grp', 'dp'), None, 'kv'), parts along dimension 0, may hold values from -4 to 4
- prev_forget: float32 [256, 4, 16], P(('grp', 'dp'), None, 'kv'), parts along dimension 0, may hold values from -2 to -0.02
- accepted: int32 [256], P(('grp', 'dp')), parts along dimension 0, may hold values from 0 to 4
Outputs:
- mixed: bfloat16 [256, 4, 4096], P(('grp', 'dp'), None, ('kv', 'tp')), parts along dimension 0
- new_memory: float32 [256, 16, 128, 64], P(('grp', 'dp'), 'kv', 'tp'), parts along dimension 0
- new_normalizer: float32 [256, 16, 64], P(('grp', 'dp'), 'kv'), parts along dimension 0
- new_stabilizer: float32 [256, 16], P(('grp', 'dp'), 'kv'), parts along dimension 0
- new_keys: bfloat16 [256, 4, 16, 64], P(('grp', 'dp'), None, 'kv'), parts along dimension 0
- new_values: bfloat16 [256, 4, 16, 128], P(('grp', 'dp'), None, 'kv', 'tp'), parts along dimension 0
- new_input: float32 [256, 4, 16], P(('grp', 'dp'), None, 'kv'), parts along dimension 0
- new_forget: float32 [256, 4, 16], P(('grp', 'dp'), None, 'kv'), parts along dimension 0
There are 2 independent parts, one for each index of `grp`. A program takes and returns all parts, laid end to end along the dimension named above; an argument that names none is the same for every part. Nothing has to cross between parts.
All inputs are finite; a program needn't handle non-finite values.
Results may differ from a plain program's by a relative error of at most 0.038.
Values may be sent and summed in bfloat16 or wider, within the bound.
A program may use at most 128 MiB of HBM per device.

v0:
```python
import jax
import jax.numpy as jnp
from jax import lax
from jax.sharding import PartitionSpec as P

EPS = 1e-06
FAR_NEGATIVE = -1e30
HIGHEST_PRECISION = lax.Precision.HIGHEST


def recurrent(
    query_f, key_all, value_all, gate_in, gate_forget, accepted, memory, normalizer, stabilizer
):
    proposals = query_f.shape[1]
    total_span = key_all.shape[1]
    position = jnp.arange(total_span, dtype=jnp.int32)
    dropped = (position[None, :] < proposals) & (position[None, :] >= accepted[:, None])
    forget = jnp.where(dropped[:, :, None], 0.0, gate_forget)
    inflow = jnp.where(dropped[:, :, None], FAR_NEGATIVE, gate_in)
    running = jnp.cumsum(forget, axis=1)
    latest = running[:, proposals:]
    spread = latest[:, :, None, :] - running[:, None, :, :] + inflow[:, None, :, :]
    causal = position[None, :] <= (proposals + jnp.arange(proposals, dtype=jnp.int32))[:, None]
    spread = jnp.where(causal[None, :, :, None], spread, FAR_NEGATIVE)
    carried = latest + stabilizer[:, None, :]
    ceiling = jnp.maximum(jnp.max(spread, axis=2), carried)
    scores = jnp.einsum("sthk,suhk->stuh", query_f, key_all, precision=HIGHEST_PRECISION)
    weights = jnp.exp(spread - ceiling[:, :, None, :]) * scores
    carry_scale = jnp.exp(carried - ceiling)
    numerator = jnp.einsum("stuh,suhv->sthv", weights, value_all, precision=HIGHEST_PRECISION)
    numerator = numerator + carry_scale[..., None] * jnp.einsum(
        "shvk,sthk->sthv", memory, query_f, precision=HIGHEST_PRECISION
    )
    denominator = jnp.sum(weights, axis=2) + carry_scale * jnp.einsum(
        "shk,sthk->sth", normalizer, query_f, precision=HIGHEST_PRECISION
    )
    cell_out = numerator / jnp.maximum(jnp.abs(denominator), jnp.exp(-ceiling))[..., None]
    boundary = running[:, proposals - 1]
    reached = boundary[:, None, :] - running[:, :proposals] + inflow[:, :proposals]
    new_stabilizer = jnp.maximum(boundary + stabilizer, jnp.max(reached, axis=1))
    decay_old = jnp.exp(boundary + stabilizer - new_stabilizer)
    shares = jnp.exp(reached - new_stabilizer[:, None, :])
    new_memory = decay_old[:, :, None, None] * memory + jnp.einsum(
        "sjh,sjhv,sjhk->shvk",
        shares,
        value_all[:, :proposals],
        key_all[:, :proposals],
        precision=HIGHEST_PRECISION,
    )
    new_normalizer = decay_old[:, :, None] * normalizer + jnp.einsum(
        "sjh,sjhk->shk", shares, key_all[:, :proposals], precision=HIGHEST_PRECISION
    )
    return (cell_out, new_memory, new_normalizer, new_stabilizer)


def shards(
    tokens,
    norm_gain,
    w_query,
    w_key,
    w_value,
    w_outgate,
    w_input,
    w_forget,
    forget_bias,
    head_gain,
    w_out,
    memory,
    normalizer,
    stabilizer,
    prev_keys,
    prev_values,
    prev_input,
    prev_forget,
    accepted,
):
    sequences, proposals, columns = tokens.shape
    model_width = w_query.shape[0]
    local_heads = w_query.shape[1]
    key_size = w_query.shape[2]
    value_part = w_value.shape[2]
    token_rows = sequences * proposals
    head_start = lax.axis_index("kv") * local_heads
    value_start = lax.axis_index("tp") * value_part
    input_cols = lax.dynamic_slice_in_dim(w_input, head_start, local_heads, 1)
    forget_cols = lax.dynamic_slice_in_dim(w_forget, head_start, local_heads, 1)
    forget_shift = lax.dynamic_slice_in_dim(forget_bias, head_start, local_heads, 0)
    gain_block = lax.dynamic_slice(head_gain, (head_start, value_start), (local_heads, value_part))
    gathered = lax.all_gather(tokens, ("kv", "tp"), axis=2, tiled=True)
    as_float = gathered.astype(jnp.float32)
    inv_scale = lax.rsqrt(jnp.mean(as_float * as_float, axis=-1, keepdims=True) + EPS)
    normed = (as_float * inv_scale * norm_gain).astype(jnp.bfloat16)
    normed = normed.reshape(token_rows, model_width)

    def project(weight):
        return jnp.dot(normed, weight.reshape(model_width, -1), preferred_element_type=jnp.float32)

    queries = (
        project(w_query).astype(jnp.bfloat16).reshape(sequences, proposals, local_heads, key_size)
    )
    new_keys = (
        project(w_key).astype(jnp.bfloat16).reshape(sequences, proposals, local_heads, key_size)
    )
    new_values = (
        project(w_value).astype(jnp.bfloat16).reshape(sequences, proposals, local_heads, value_part)
    )
    out_gate = project(w_outgate).reshape(sequences, proposals, local_heads, value_part)
    new_input = project(input_cols).reshape(sequences, proposals, local_heads)
    new_forget = jax.nn.log_sigmoid(
        project(forget_cols).reshape(sequences, proposals, local_heads) + forget_shift
    )
    query_f = queries.astype(jnp.float32) * key_size ** (-0.5)
    key_all = jnp.concatenate([prev_keys, new_keys], axis=1).astype(jnp.float32)
    value_all = jnp.concatenate([prev_values, new_values], axis=1).astype(jnp.float32)
    gate_in = jnp.concatenate([prev_input, new_input], axis=1)
    gate_forget = jnp.concatenate([prev_forget, new_forget], axis=1)
    cell_out, new_memory, new_normalizer, new_stabilizer = recurrent(
        query_f, key_all, value_all, gate_in, gate_forget, accepted, memory, normalizer, stabilizer
    )
    head_squares = lax.psum(jnp.sum(cell_out * cell_out, axis=-1), "tp")
    full_values = value_part * lax.axis_size("tp")
    inv_head = lax.rsqrt(head_squares / full_values + EPS)
    gated = (jax.nn.sigmoid(out_gate) * cell_out * inv_head[..., None] * gain_block).astype(
        jnp.bfloat16
    )
    flat_rows = gated.reshape(token_rows, local_heads * value_part)
    out_block = lax.all_to_all(
        w_out.reshape(1, local_heads * value_part, model_width),
        ("kv", "tp"),
        split_axis=2,
        concat_axis=0,
        tiled=True,
    )
    summed = jnp.einsum(
        "gtc,gcd->td",
        lax.all_gather(
            flat_rows.reshape(1, token_rows, local_heads * value_part),
            ("kv", "tp"),
            axis=0,
            tiled=True,
        ),
        out_block,
        preferred_element_type=jnp.float32,
    )
    mixed = summed.astype(jnp.bfloat16).reshape(sequences, proposals, out_block.shape[2])
    return (
        mixed,
        new_memory,
        new_normalizer,
        new_stabilizer,
        new_keys,
        new_values,
        new_input,
        new_forget,
    )


def solution(mesh):
    return jax.shard_map(
        shards,
        mesh=mesh,
        in_specs=(
            P(("grp", "dp"), None, ("kv", "tp")),
            P(),
            P(None, "kv", None),
            P(None, "kv", None),
            P(None, "kv", "tp"),
            P(None, "kv", "tp"),
            P(),
            P(),
            P(),
            P(),
            P("kv", "tp", None),
            P(("grp", "dp"), "kv", "tp", None),
            P(("grp", "dp"), "kv", None),
            P(("grp", "dp"), "kv"),
            P(("grp", "dp"), None, "kv", None),
            P(("grp", "dp"), None, "kv", "tp"),
            P(("grp", "dp"), None, "kv"),
            P(("grp", "dp"), None, "kv"),
            P(("grp", "dp")),
        ),
        out_specs=(
            P(("grp", "dp"), None, ("kv", "tp")),
            P(("grp", "dp"), "kv", "tp", None),
            P(("grp", "dp"), "kv", None),
            P(("grp", "dp"), "kv"),
            P(("grp", "dp"), None, "kv", None),
            P(("grp", "dp"), None, "kv", "tp"),
            P(("grp", "dp"), None, "kv"),
            P(("grp", "dp"), None, "kv"),
        ),
        check_vma=False,
    )
```

profile of v0, /device:TPU:0, one launch (start us, length us, event | category | flops | bytes accessed | tf_op | source)
XLA Modules:
  0.0 165.0 jit_solution(10992848654207811287)
XLA Ops:
  7.9 10.0 %copy.164 = bf16[1,256,4096]{1,0,2:T(2,128)(2,1)} copy(bf16[1,256,4096]{2,1,0:T(8,128)(2,1)} %bitcast.117) | data formatting | bytes 4194304 | tf_op jit(solution)/shard_map/reshape | solution.py:128
  18.4 22.9 %reduce = bf16[4096,256]{1,0:T(8,128)(2,1)} reduce(bf16[4096,1,256]{2,1,0:T(2,128)(2,1)} %bitcast.114, bf16[]{:T(256)} %broadcast.99), dimensions={1}, to_apply=%bitcast.96.reduce_sub_computation | reduce | bytes 4194306
  41.3 5.8 %reshape.176 = bf16[8,2,65536]{2,1,0:T(2,128)(2,1)} reshape(bf16[4096,256]{1,0:T(8,128)(2,1)} %reduce) | data formatting | bytes 4194304
  47.1 6.5 %all-to-all-start = ((bf16[8,2,65536]{2,1,0:T(2,128)(2,1)}), bf16[8,2,65536]{2,1,0:T(2,128)(2,1)}, u32[]{:S(2)}, u32[]{:S(2)}) async-start(bf16[8,2,65536]{2,1,0:T(2,128)(2,1)} %reshape.176), calls=%async_computation | async-start | bytes 4194304 | tf_op jit(solution)/shard_map/all_to_all | solution.py:127
  53.8 0.8 copy.147
  54.7 1.3 dynamic_slice.15
  56.2 2.9 %fusion = f32[64,4]{1,0:T(8,128)S(1)} fusion(bf16[64,4,4096]{2,1,0:T(4,128)(2,1)} %all-gather.3.cloned.1.call-done), kind=kLoop, calls=%fused_computation.3 | loop fusion | flops 3145472 | bytes 2098176 | tf_op jit(solution)/shard_map/reduce_sum | solution.py:91
  59.1 1.9 %fusion.2 = bf16[64,4,4096]{2,1,0:T(4,128)(2,1)S(1)} fusion(bf16[64,4,4096]{2,1,0:T(4,128)(2,1)S(1)} %copy-done.1, f32[4096]{0:T(1024)S(1)} %copy-done.19, f32[64,4]{1,0:T(8,128)S(1)} %add_rsqrt_fusion), kind=kLoop, calls=%fused_computation.5 | loop fusion | flops 4194304 | bytes 4211712 | tf_op jit(solution)/shard_map/convert_element_type | solution.py:92
  61.1 1.3 copy-done.2
  62.4 3.2 %fusion.90 = f32[64,4,4]{0,2,1:T(4,128)S(1)} fusion(bf16[4096,16]{0,1:T(8,128)(2,1)} %param.26, s32[]{:T(128)S(6)} %select_n.29, bf16[64,4,4096]{2,1,0:T(4,128)(2,1)S(1)} %fusion.2, f32[4]{0:T(128)S(1)} %dynamic_slice.13), kind=kOutput, calls=%fused_computation.66 | convolution fusion | flops 8397824 | bytes 2134036 | tf_op jit(solution)/shard_map/dot_general | solution.py:96
  66.2 4.0 %reshape.159 = bf16[256,4096]{1,0:T(8,128)(2,1)} reshape(bf16[64,4,4096]{2,1,0:T(4,128)(2,1)} %copy-done.2) | data formatting | bytes 4194304 | tf_op jit(solution)/shard_map/reshape | solution.py:93
  70.3 3.9 %fusion.8 = f32[64,4,4]{0,2,1:T(4,128)S(1)} fusion(bf16[64,4,4096]{2,1,0:T(4,128)(2,1)} %copy-done.2, bf16[4096,16]{0,1:T(8,128)(2,1)} %param.25, s32[]{:T(128)S(6)} %select_n.29), kind=kOutput, calls=%fused_computation.11 | convolution fusion | flops 8388608 | bytes 2134020 | tf_op jit(solution)/shard_map/dot_general | solution.py:96
  77.3 2.3 %fusion.35 = f32[256,256]{1,0:T(8,128)S(1)} fusion(bf16[256,4096]{1,0:T(8,128)(2,1)} %reshape.159, bf16[4096,256]{0,1:T(8,128)(2,1)S(1)} %bitcast.113), kind=kOutput, calls=%fused_computation.24 | convolution fusion | flops 537067520 | bytes 4456448 | tf_op jit(solution)/shard_map/dot_general | solution.py:96
  79.8 3.6 %convolution_convert_fusion.1 = bf16[256,256]{1,0:T(8,128)(2,1)} fusion(bf16[256,4096]{1,0:T(8,128)(2,1)} %reshape.159, bf16[4096,256]{0,1:T(8,128)(2,1)} %bitcast.121), kind=kOutput, calls=%fused_computation.25 | convolution fusion | flops 536936448 | bytes 4325376 | tf_op jit(solution)/shard_map/dot_general | solution.py:96
  83.5 1.1 reshape.163
  84.7 3.7 %convolution_convert_fusion.2 = bf16[256,256]{1,0:T(8,128)(2,1)} fusion(bf16[256,4096]{1,0:T(8,128)(2,1)} %reshape.159, bf16[4096,256]{0,1:T(8,128)(2,1)} %bitcast.122), kind=kOutput, calls=%fused_computation.26 | convolution fusion | flops 536936448 | bytes 4325376 | tf_op jit(solution)/shard_map/dot_general | solution.py:96
  88.4 3.1 %fusion.111 = (f32[64,4,4]{1,2,0:T(4,128)}, f32[64,4,8,4]{2,1,3,0:T(4,128)}) fusion(f32[64,4,4,64]{3,2,1,0:T(4,128)S(1)} %mul.94, bf16[64,4,4,64]{3,1,2,0:T(4,128)(2,1)S(1)} %copy.157, bf16[64,4,4,64]{3,1,2,0:T(4,128)(2,1)S(1)} %copy.156, f32[64,4,4]{1,2,0:T(4,128)S(1)} %copy-done.16, f32[64,8,4]{1,2,0:T(4,128)S(1)} %copy.153, f32[64,8,4]{1,2,0:T(4,128)S(1)} %copy.151, ...), kind=kOutput, calls=%fused_computation.95 | convolution fusion | flops 6863872 | bytes 585760 | tf_op jit(solution)/shard_map/sthk,suhk->stuh/dot_general | solution.py:27
  91.5 1.8 %fusion.80 = f32[64,4,1,4]{3,2,1,0:T(1,128)S(1)} fusion(f32[64,4,64,1]{2,3,1,0:T(1,128)S(1)} %bitcast.118, f32[64,4,4,64]{3,2,1,0:T(4,128)S(1)} %mul.94), kind=kOutput, calls=%fused_computation.51 | convolution fusion | flops 786432 | bytes 331776 | tf_op jit(solution)/shard_map/shk,sthk->sth/dot_general | solution.py:34
  93.3 1.1 reshape.161
  95.2 1.0 copy.162
  96.4 2.4 %fusion.67 = f32[64,4,64,4]{2,3,1,0:T(4,128)S(1)} fusion(f32[64,4,8,4]{2,1,3,0:T(4,128)} %get-tuple-element.16, bf16[64,4,4,64]{3,1,2,0:T(4,128)(2,1)} %copy.148, bf16[64,4,4,64]{3,1,2,0:T(4,128)(2,1)} %copy.147), kind=kOutput, calls=%fused_computation.34 | convolution fusion | flops 6815744 | bytes 557056 | tf_op jit(solution)/shard_map/stuh,suhv->sthv/dot_general | solution.py:30
  98.9 15.6 %fusion.78 = f32[64,4,4,64]{3,2,1,0:T(4,128)S(1)} fusion(f32[64,4,64,64]{3,2,1,0:T(8,128)} %param.30, f32[64,4,4,64]{3,2,1,0:T(4,128)S(1)} %mul.94), kind=kOutput, calls=%fused_computation.49 | convolution fusion | flops 50331648 | bytes 4718592 | tf_op jit(solution)/shard_map/shvk,sthk->sthv/dot_general | solution.py:31
  115.9 2.6 %psum.7 = f32[64,4,4]{0,2,1:T(4,128)S(1)} all-reduce(f32[64,4,4]{0,2,1:T(4,128)S(1)} %multiply_reduce_fusion), channel_id=1, replica_groups=mesh['grp'=2,'dp'=2,'kv'=4,'tp'=2] {'tp'}, use_global_device_ids=true, to_apply=%region_5.6 | all-reduce | flops 1024 | bytes 8192 | tf_op jit(solution)/shard_map/psum | solution.py:120
  118.5 3.1 %fusion.126 = bf16[64,4,4096,1]{2,1,0,3:T(4,128)(2,1)S(1)} fusion(f32[4096]{0:T(1024)S(1)} %copy-done.20, f32[64,4]{1,0:T(8,128)S(1)} %copy-done.10, bf16[64,4,4096]{2,1,0:T(4,128)(2,1)} %all-gather.3.cloned.1.call-done), kind=kLoop, calls=%fused_computation.97 | loop fusion | flops 4194304 | bytes 4211712 | tf_op jit(solution)/shard_map/convert_element_type | solution.py:92
  121.7 2.1 %fusion.56 = bf16[64,4,4,64]{3,0,2,1:T(8,128)(2,1)S(1)} fusion(bf16[4096,4,64]{0,2,1:T(8,128)(2,1)S(1)} %copy-done.35, bf16[64,4,4096,1]{2,1,0,3:T(4,128)(2,1)S(1)} %fusion.126, f32[4,64]{1,0:T(4,128)S(1)} %copy-done.31, f32[64,4,4]{0,2,1:T(4,128)S(1)} %add_rsqrt_fusion.1, f32[64,4,4]{0,2,1:T(4,128)S(1)} %get-tuple-element.10, ...), kind=kOutput, calls=%fused_computation.31 | convolution fusion | flops 537526272 | bytes 4862976 | tf_op jit(solution)/shard_map/dot_general | solution.py:96
  124.1 0.9 reshape_reshape.3
  125.0 7.0 %reshape.177 = bf16[4096,1,256]{2,1,0:T(2,128)(2,1)} reshape(bf16[8,2,65536]{2,1,0:T(2,128)(2,1)} %all-to-all-done) | data formatting | bytes 4194304
  132.0 3.9 %copy.178 = bf16[1,256,4096]{1,2,0:T(8,128)(2,1)} copy(bf16[1,256,4096]{1,0,2:T(2,128)(2,1)} %bitcast.115) | data formatting | bytes 4194304
  135.9 4.0 %copy.165 = bf16[1,256,8,512]{3,1,2,0:T(8,128)(2,1)} copy(bf16[1,256,8,512]{1,3,2,0:T(8,128)(2,1)} %bitcast.116) | data formatting | bytes 4194304 | tf_op jit(solution)/shard_map/all_to_all | solution.py:127
  140.3 1.0 fusion.112
  142.4 12.3 %multiply_add_fusion = f32[64,4,64,64]{3,2,1,0:T(8,128)} fusion(f32[64,4,64,64]{3,2,1,0:T(8,128)} %param.30, f32[64,4]{1,0:T(8,128)S(1)} %copy.166, bf16[64,4,4,64]{3,1,2,0:T(4,128)(2,1)S(1)} %copy.156, f32[64,4,4,64]{3,2,1,0:T(4,128)S(1)} %convert_multiply_fusion.2), kind=kOutput, calls=%fused_computation | convolution fusion | flops 52428800 | bytes 8782848 | tf_op jit(solution)/shard_map/sjh,sjhv,sjhk->shvk/dot_general | solution.py:43
  154.7 2.6 %fusion.31 = bf16[256,512]{1,0:T(8,128)(2,1)S(1)} fusion(bf16[8,256,256]{2,1,0:T(8,128)(2,1)} %all-gather.5.cloned.1.call-done, bf16[1,256,8,512]{3,1,2,0:T(8,128)(2,1)} %copy.165), kind=kOutput, calls=%fused_computation.21 | convolution fusion | flops 537001984 | bytes 3407872 | tf_op jit(solution)/shard_map/gtc,gcd->td/dot_general | solution.py:134
  (114 shorter events, 10.6 us)
Async XLA Ops:
  7.2 70.1 %copy-start = (bf16[4096,4,64]{0,2,1:T(8,128)(2,1)S(1)}, bf16[4096,4,64]{0,2,1:T(8,128)(2,1)}, u32[]{:S(2)}) copy-start(bf16[4096,4,64]{0,2,1:T(8,128)(2,1)} %param.21) | copy-start | bytes 6291460
  7.2 49.0 %all-gather.3.cloned.1.call-start = ((), (), s32[]{:S(2)}) async-start(), calls=%async_computation.1 | async-start | bytes 2359296 | tf_op jit(solution)/shard_map/all_gather | solution.py:89
  47.1 6.6 %copy-start.11 = (bf16[64,4,4,64]{3,2,1,0:T(4,128)(2,1)S(1)}, bf16[64,4,4,64]{3,2,1,0:T(4,128)(2,1)}, u32[]{:S(2)}) copy-start(bf16[64,4,4,64]{3,2,1,0:T(4,128)(2,1)} %param.33) | copy-start | bytes 393220
  47.1 6.7 %copy-start.5 = (bf16[64,4,4,64]{3,2,1,0:T(4,128)(2,1)S(1)}, bf16[64,4,4,64]{3,2,1,0:T(4,128)(2,1)}, u32[]{:S(2)}) copy-start(bf16[64,4,4,64]{3,2,1,0:T(4,128)(2,1)} %param.34) | copy-start | bytes 393220
  47.1 7.5 %copy-start.36 = (f32[16]{0:T(128)S(1)}, f32[16]{0:T(128)}, u32[]{:S(2)}) copy-start(f32[16]{0:T(128)} %param.27) | copy-start | bytes 196
  47.1 9.0 %copy-start.34 = (s32[64]{0:T(128)S(1)}, s32[64]{0:T(128)}, u32[]{:S(2)}) copy-start(s32[64]{0:T(128)} %param.37) | copy-start | bytes 772
  47.1 77.9 %all-to-all-start = ((bf16[8,2,65536]{2,1,0:T(2,128)(2,1)}), bf16[8,2,65536]{2,1,0:T(2,128)(2,1)}, u32[]{:S(2)}, u32[]{:S(2)}) async-start(bf16[8,2,65536]{2,1,0:T(2,128)(2,1)} %reshape.176), calls=%async_computation | async-start | bytes 4194304 | tf_op jit(solution)/shard_map/all_to_all | solution.py:127
  53.6 5.5 %copy-start.19 = (f32[4096]{0:T(1024)S(1)}, f32[4096]{0:T(1024)}, u32[]{:S(2)}) copy-start(f32[4096]{0:T(1024)} %param.20) | copy-start | bytes 49156
  53.6 101.1 %all-gather.5.cloned.1.call-start = ((), (), s32[]{:S(2)}) async-start(), calls=%async_computation.2 | async-start | bytes 1179648 | tf_op jit(solution)/shard_map/all_gather | solution.py:136
  56.1 18.9 %copy-start.32 = (pred[4,8]{1,0:T(4,128)(4,1)}, pred[4,8]{1,0:T(4,128)(4,1)S(1)}, u32[]{:S(2)}) copy-start(pred[4,8]{1,0:T(4,128)(4,1)S(1)} %iota_compare_fusion.1) | copy-start | bytes 100
  56.2 2.9 %copy-start.1 = (bf16[64,4,4096]{2,1,0:T(4,128)(2,1)S(1)}, bf16[64,4,4096]{2,1,0:T(4,128)(2,1)}, u32[]{:S(2)}) copy-start(bf16[64,4,4096]{2,1,0:T(4,128)(2,1)} %all-gather.3.cloned.1.call-done) | copy-start | bytes 6291460
  62.4 3.2 %copy-start.27 = (f32[64,4,4]{0,2,1:T(4,128)S(1)}, f32[64,4,4]{0,2,1:T(4,128)}, u32[]{:S(2)}) copy-start(f32[64,4,4]{0,2,1:T(4,128)} %param.36) | copy-start | bytes 12292
  66.2 9.7 %copy-start.23 = (f32[64,4]{0,1:T(4,128)}, f32[64,4]{0,1:T(4,128)S(1)}, u32[]{:S(2)}) copy-start(f32[64,4]{0,1:T(4,128)S(1)} %slice_bitcast_fusion) | copy-start | bytes 3076
  70.2 4.6 %copy-start.28 = (f32[64,4,4]{0,2,1:T(4,128)S(1)}, f32[64,4,4]{0,2,1:T(4,128)}, u32[]{:S(2)}) copy-start(f32[64,4,4]{0,2,1:T(4,128)} %param.35) | copy-start | bytes 12292
  70.2 5.7 %copy-start.21 = (f32[64,4]{0,1:T(4,128)S(1)}, f32[64,4]{0,1:T(4,128)}, u32[]{:S(2)}) copy-start(f32[64,4]{0,1:T(4,128)} %param.32) | copy-start | bytes 3076
  84.5 3.8 %copy-start.7 = (bf16[64,4,4,64]{3,2,1,0:T(4,128)(2,1)}, bf16[64,4,4,64]{3,2,1,0:T(4,128)(2,1)S(1)}, u32[]{:S(2)}) copy-start(bf16[64,4,4,64]{3,2,1,0:T(4,128)(2,1)S(1)} %reshape.163) | copy-start | bytes 393220
  84.7 3.7 %copy-start.16 = (f32[64,4,4]{1,2,0:T(4,128)S(1)}, f32[64,4,4]{1,2,0:T(4,128)}, u32[]{:S(2)}) copy-start(f32[64,4,4]{1,2,0:T(4,128)} %copy.155) | copy-start | bytes 12292
  84.7 3.7 %copy-start.33 = (pred[4,8]{1,0:T(4,128)(4,1)S(1)}, pred[4,8]{1,0:T(4,128)(4,1)}, u32[]{:S(2)}) copy-start(pred[4,8]{1,0:T(4,128)(4,1)} %copy-done.32) | copy-start | bytes 100
  88.3 3.1 %copy-start.14 = (f32[64,4,64]{2,1,0:T(4,128)S(1)}, f32[64,4,64]{2,1,0:T(4,128)}, u32[]{:S(2)}) copy-start(f32[64,4,64]{2,1,0:T(4,128)} %param.31) | copy-start | bytes 196612
  91.4 4.9 %copy-start.22 = (f32[64,4]{0,1:T(4,128)S(1)}, f32[64,4]{0,1:T(4,128)}, u32[]{:S(2)}) copy-start(f32[64,4]{0,1:T(4,128)} %param.32) | copy-start | bytes 3076
  91.4 4.9 %copy-start.26 = (f32[64,4]{0,1:T(4,128)S(1)}, f32[64,4]{0,1:T(4,128)}, u32[]{:S(2)}) copy-start(f32[64,4]{0,1:T(4,128)} %get-tuple-element.13) | copy-start | bytes 3076
  91.4 4.9 %copy-start.13 = (f32[64,8,4]{0,2,1:T(4,128)S(1)}, f32[64,8,4]{0,2,1:T(4,128)}, u32[]{:S(2)}) copy-start(f32[64,8,4]{0,2,1:T(4,128)} %copy-done.12) | copy-start | bytes 24580
  91.4 4.9 %copy-start.18 = (f32[64,4,4]{0,2,1:T(4,128)S(1)}, f32[64,4,4]{0,2,1:T(4,128)}, u32[]{:S(2)}) copy-start(f32[64,4,4]{0,2,1:T(4,128)} %copy-done.17) | copy-start | bytes 12292
  91.4 4.9 %copy-start.24 = (f32[64,4]{0,1:T(4,128)S(1)}, f32[64,4]{0,1:T(4,128)}, u32[]{:S(2)}) copy-start(f32[64,4]{0,1:T(4,128)} %copy-done.23) | copy-start | bytes 3076
  96.3 18.1 %copy-start.25 = (f32[64,4]{0,1:T(4,128)}, f32[64,4]{0,1:T(4,128)S(1)}, u32[]{:S(2)}) copy-start(f32[64,4]{0,1:T(4,128)S(1)} %get-tuple-element.9) | copy-start | bytes 3076
  98.8 19.7 %copy-start.10 = (f32[64,4]{1,0:T(8,128)S(1)}, f32[64,4]{1,0:T(8,128)}, u32[]{:S(2)}) copy-start(f32[64,4]{1,0:T(8,128)} %copy-done.9) | copy-start | bytes 3076
  98.9 19.7 %copy-start.20 = (f32[4096]{0:T(1024)S(1)}, f32[4096]{0:T(1024)}, u32[]{:S(2)}) copy-start(f32[4096]{0:T(1024)} %param.20) | copy-start | bytes 49156
  118.5 3.2 %copy-start.4 = (f32[64,4,4,64]{3,2,1,0:T(4,128)S(1)}, f32[64,4,4,64]{3,2,1,0:T(4,128)}, u32[]{:S(2)}) copy-start(f32[64,4,4,64]{3,2,1,0:T(4,128)} %copy-done.3) | copy-start | bytes 786436
  118.5 3.2 %copy-start.31 = (f32[4,64]{1,0:T(4,128)S(1)}, f32[4,64]{1,0:T(4,128)}, u32[]{:S(2)}) copy-start(f32[4,64]{1,0:T(4,128)} %dynamic_slice.15) | copy-start | bytes 3076
  118.5 3.2 %copy-start.35 = (bf16[4096,4,64]{0,2,1:T(8,128)(2,1)S(1)}, bf16[4096,4,64]{0,2,1:T(8,128)(2,1)}, u32[]{:S(2)}) copy-start(bf16[4096,4,64]{0,2,1:T(8,128)(2,1)} %param.24) | copy-start | bytes 6291460
  135.9 5.3 %copy-start.15 = (f32[64,4,64]{2,1,0:T(4,128)S(1)}, f32[64,4,64]{2,1,0:T(4,128)}, u32[]{:S(2)}) copy-start(f32[64,4,64]{2,1,0:T(4,128)} %param.31) | copy-start | bytes 196612
  135.9 6.1 %copy-start.6 = (bf16[64,4,4,64]{3,2,1,0:T(4,128)(2,1)S(1)}, bf16[64,4,4,64]{3,2,1,0:T(4,128)(2,1)}, u32[]{:S(2)}) copy-start(bf16[64,4,4,64]{3,2,1,0:T(4,128)(2,1)} %param.34) | copy-start | bytes 393220
  (8 other events, 10.5 us)
Sparse Core Ops, SparseCore 0:
  9.6 33.3 all-gather.2
  125.1 23.5 all-gather.4
where the time goes:
time: 166 us; the launch traced here: 165 us
  matrix products  57.6 us (35%)
  local copies, waits for them, and re-layouts  48.6 us (29%)
  other arithmetic  34.2 us (21%)
  between operations  14.6 us (9%)
  starting transfers between devices  6.58 us (4%)
  blocking collectives  2.62 us (2%)
    unnamed x1, other arithmetic  22.9 us
    unnamed x80, local copies, waits for them, and re-layouts  21.5 us
    dot_general x6, matrix products, project(): jnp.dot(normed, weight.reshape(model_width, -1), preferred_element_type=j...  18.8 us
    dot_general x1, matrix products, recurrent(): jnp.einsum('shvk,sthk->sthv', memory, query_f, precision=HIGHEST_PRECISION)  15.6 us
    dot_general x1, matrix products, recurrent(): jnp.einsum('sjh,sjhv,sjhk->shvk', shares, value_all[:, :proposals], key_a...  12.3 us
    reshape x1, local copies, waits for them, and re-layouts, shards(): w_out.reshape(1, local_heads * value_part, model_width)  9.96 us
    all_to_all x1, starting transfers between devices, shards(): lax.all_to_all(w_out.reshape(1, local_heads * value_part, model_width), (...  6.5 us
    convert_element_type x2, other arithmetic, shards(): normed = (as_float * inv_scale * norm_gain).astype(jnp.bfloat16)  5.06 us
  transfers between devices with their start and end apart: 3, of which 0 were waited for; matrix products, arithmetic and copies ran while one was open for 81% of the time, Pallas kernels for 0%

commit v1 on v0

--- a/solution.py
+++ b/solution.py
@@ -2,6 +2,7 @@
 import jax.numpy as jnp
 from jax import lax
 from jax.sharding import PartitionSpec as P
+from jax.lax import all_to_all, axis_size
 
 EPS = 1e-06
 FAR_NEGATIVE = -1e30
@@ -74,6 +75,19 @@
     prev_forget,
     accepted,
 ):
+
+    def shape_sheet(x_local):
+        back = jnp.concatenate(
+            all_to_all(
+                jnp.stack(jnp.split(x_local, axis_size(("kv", "tp")), 2)),
+                axis_name=("kv", "tp"),
+                concat_axis=0,
+                split_axis=0,
+            ),
+            0,
+        )
+        return back
+
     sequences, proposals, columns = tokens.shape
     model_width = w_query.shape[0]
     local_heads = w_query.shape[1]
@@ -124,13 +138,7 @@
         jnp.bfloat16
     )
     flat_rows = gated.reshape(token_rows, local_heads * value_part)
-    out_block = lax.all_to_all(
-        w_out.reshape(1, local_heads * value_part, model_width),
-        ("kv", "tp"),
-        split_axis=2,
-        concat_axis=0,
-        tiled=True,
-    )
+    out_block = shape_sheet(w_out.reshape(1, local_heads * value_part, model_width))
     summed = jnp.einsum(
         "gtc,gcd->td",
         lax.all_gather(

time: 166 us -> 160 us (0.964)
  waiting for transfers between devices: 0.7 us -> 40.1 us
  local copies, waits for them, and re-layouts: 48.6 us -> 26.9 us
  other arithmetic: 34.2 us -> 12.6 us
    all_gather x1, waiting for transfers between devices: 0.01 us -> 31.9 us  [shards(): gathered = lax.all_gather(tokens, ('kv', 'tp'), axis=2, tiled=True)]
    unnamed x1 -> x0, other arithmetic: 22.9 us -> none
    reshape x1 -> x0, local copies, waits for them, and re-layouts: 9.96 us -> none  [shards(): w_out.reshape(1, local_heads * value_part, model_width)]
    unnamed x80 -> x91, local copies, waits for them, and re-layouts: 21.5 us -> 12.7 us
    all_gather x1, waiting for transfers between devices: 0.01 us -> 7.44 us  [shards(): lax.all_gather(flat_rows.reshape(1, token_rows, local_heads * value_part)...]
    all_to_all x1 -> x0, local copies, waits for them, and re-layouts: 3.98 us -> none  [shards(): lax.all_to_all(w_out.reshape(1, local_heads * value_part, model_width), (...]
  transfers between devices with their start and end apart: 3 -> 3, of which waited for: 0 -> 2; matrix products, arithmetic and copies ran while one was open for 81% -> 56% of each run, Pallas kernels for 0% -> 0%
where the time goes in v1:
time: 160 us
  matrix products  56.2 us (35%)
  waiting for transfers between devices  40.1 us (25%)
  local copies, waits for them, and re-layouts  26.9 us (17%)
  between operations  14.7 us (9%)
  other arithmetic  12.6 us (8%)
  starting transfers between devices  6.58 us (4%)
  blocking collectives  2.5 us (2%)
    all_gather x1, waiting for transfers between devices, shards(): gathered = lax.all_gather(tokens, ('kv', 'tp'), axis=2, tiled=True)  31.9 us
    dot_general x6, matrix products, project(): jnp.dot(normed, weight.reshape(model_width, -1), preferred_element_type=j...  18.1 us
    dot_general x1, matrix products, recurrent(): jnp.einsum('shvk,sthk->sthv', memory, query_f, precision=HIGHEST_PRECISION)  15.7 us
    unnamed x91, local copies, waits for them, and re-layouts  12.7 us
    dot_general x1, matrix products, recurrent(): jnp.einsum('sjh,sjhv,sjhk->shvk', shares, value_all[:, :proposals], key_a...  12.3 us
    all_gather x1, waiting for transfers between devices, shards(): lax.all_gather(flat_rows.reshape(1, token_rows, local_heads * value_part)...  7.44 us
    all_to_all x1, starting transfers between devices, shape_sheet(): all_to_all(jnp.stack(jnp.split(x_local, axis_size(('kv', 'tp')), 2)), axi...  6.5 us
    convert_element_type x2, other arithmetic, shards(): normed = (as_float * inv_scale * norm_gain).astype(jnp.bfloat16)  5.06 us
  transfers between devices with their start and end apart: 3, of which 2 were waited for; matrix products, arithmetic and copies ran while one was open for 56% of the time, Pallas kernels for 0%

profile of v1, /device:TPU:0, one launch (start us, length us, event | category | flops | bytes accessed | tf_op | source)
XLA Modules:
  0.0 159.5 jit_solution(5907777759631301396)
XLA Ops:
  7.9 1.8 %fusion.90 = bf16[8,1,256,512]{3,2,1,0:T(8,128)(2,1)} fusion(bf16[1,256,4096]{2,1,0:T(8,128)(2,1)} %bitcast.141), kind=kLoop, calls=%fused_computation.69 | loop fusion | bytes 524288
  9.8 1.7 %fusion.89 = bf16[8,1,256,512]{3,2,1,0:T(8,128)(2,1)} fusion(bf16[8,1,256,512]{3,2,1,0:T(8,128)(2,1)} %fusion.90, bf16[1,256,4096]{2,1,0:T(8,128)(2,1)} %bitcast.142), kind=kLoop, calls=%fused_computation.67 | loop fusion | bytes 524288
  11.5 1.7 %fusion.88 = bf16[8,1,256,512]{3,2,1,0:T(8,128)(2,1)} fusion(bf16[8,1,256,512]{3,2,1,0:T(8,128)(2,1)} %fusion.89, bf16[1,256,4096]{2,1,0:T(8,128)(2,1)} %bitcast.143), kind=kLoop, calls=%fused_computation.65 | loop fusion | bytes 524288
  13.1 1.6 %fusion.87 = bf16[8,1,256,512]{3,2,1,0:T(8,128)(2,1)} fusion(bf16[8,1,256,512]{3,2,1,0:T(8,128)(2,1)} %fusion.88, bf16[1,256,4096]{2,1,0:T(8,128)(2,1)} %bitcast.144), kind=kLoop, calls=%fused_computation.63 | loop fusion | bytes 524288
  17.7 6.5 %all-to-all-start = ((bf16[8,1,256,512]{3,2,1,0:T(8,128)(2,1)}), bf16[8,1,256,512]{3,2,1,0:T(8,128)(2,1)}, u32[]{:S(2)}, u32[]{:S(2)}) async-start(bf16[8,1,256,512]{3,2,1,0:T(8,128)(2,1)} %fusion.83), calls=%async_computation | async-start | bytes 4194304 | tf_op jit(solution)/shard_map/all_to_all | solution.py:81
  24.4 0.8 copy.132
  25.3 1.3 dynamic_slice.15
  26.8 31.9 %all-gather.3.cloned.1.call-done = bf16[64,4,4096]{2,1,0:T(4,128)(2,1)} async-done(((bf16[64,4,512]{2,1,0:T(4,128)(2,1)}), bf16[64,4,4096]{2,1,0:T(4,128)(2,1)}) %all-gather.3.cloned.1.call-update) | async-done | bytes 2097168 | tf_op jit(solution)/shard_map/all_gather | solution.py:103
  58.8 2.9 %fusion = f32[64,4]{1,0:T(8,128)S(1)} fusion(bf16[64,4,4096]{2,1,0:T(4,128)(2,1)} %all-gather.3.cloned.1.call-done), kind=kLoop, calls=%fused_computation.3 | loop fusion | flops 3145472 | bytes 2098176 | tf_op jit(solution)/shard_map/reduce_sum | solution.py:105
  61.7 1.9 %fusion.2 = bf16[64,4,4096]{2,1,0:T(4,128)(2,1)S(1)} fusion(bf16[64,4,4096]{2,1,0:T(4,128)(2,1)S(1)} %copy-done.1, f32[4096]{0:T(1024)S(1)} %copy-done.22, f32[64,4]{1,0:T(8,128)S(1)} %add_rsqrt_fusion), kind=kLoop, calls=%fused_computation.5 | loop fusion | flops 4194304 | bytes 4211712 | tf_op jit(solution)/shard_map/convert_element_type | solution.py:106
  63.7 1.3 copy-done.2
  65.0 3.2 %fusion.98 = f32[64,4,4]{0,2,1:T(4,128)S(1)} fusion(bf16[4096,16]{0,1:T(8,128)(2,1)} %param.26, s32[]{:T(128)S(6)} %select_n.29, bf16[64,4,4096]{2,1,0:T(4,128)(2,1)S(1)} %fusion.2, f32[4]{0:T(128)S(1)} %dynamic_slice.13), kind=kOutput, calls=%fused_computation.82 | convolution fusion | flops 8397824 | bytes 2134036 | tf_op jit(solution)/shard_map/dot_general | solution.py:110
  68.9 4.2 %reshape.162 = bf16[256,4096]{1,0:T(8,128)(2,1)} reshape(bf16[64,4,4096]{2,1,0:T(4,128)(2,1)} %copy-done.2) | data formatting | bytes 4194304 | tf_op jit(solution)/shard_map/reshape | solution.py:107
  73.2 3.9 %fusion.8 = f32[64,4,4]{0,2,1:T(4,128)S(1)} fusion(bf16[64,4,4096]{2,1,0:T(4,128)(2,1)} %copy-done.2, bf16[4096,16]{0,1:T(8,128)(2,1)} %param.25, s32[]{:T(128)S(6)} %select_n.29), kind=kOutput, calls=%fused_computation.11 | convolution fusion | flops 8388608 | bytes 2134020 | tf_op jit(solution)/shard_map/dot_general | solution.py:110
  80.2 2.3 %fusion.35 = f32[256,256]{1,0:T(8,128)S(1)} fusion(bf16[256,4096]{1,0:T(8,128)(2,1)} %reshape.162, bf16[4096,256]{0,1:T(8,128)(2,1)S(1)} %bitcast.140), kind=kOutput, calls=%fused_computation.24 | convolution fusion | flops 537067520 | bytes 4456448 | tf_op jit(solution)/shard_map/dot_general | solution.py:110
  82.8 3.0 %convolution_convert_fusion.1 = bf16[256,256]{1,0:T(8,128)(2,1)S(1)} fusion(bf16[256,4096]{1,0:T(8,128)(2,1)} %reshape.162, bf16[4096,256]{0,1:T(8,128)(2,1)} %bitcast.152), kind=kOutput, calls=%fused_computation.25 | convolution fusion | flops 536936448 | bytes 4325376 | tf_op jit(solution)/shard_map/dot_general | solution.py:110
  86.8 3.6 %convolution_convert_fusion.2 = bf16[256,256]{1,0:T(8,128)(2,1)} fusion(bf16[256,4096]{1,0:T(8,128)(2,1)} %reshape.162, bf16[4096,256]{0,1:T(8,128)(2,1)} %bitcast.153), kind=kOutput, calls=%fused_computation.26 | convolution fusion | flops 536936448 | bytes 4325376 | tf_op jit(solution)/shard_map/dot_general | solution.py:110
  90.4 1.1 reshape.164
  91.5 0.8 copy.133
  92.3 1.3 subtract_exponential_fusion.2
  93.6 3.5 %fusion.119 = (f32[64,4,4]{1,2,0:T(4,128)S(1)}, f32[64,4,8,4]{2,1,3,0:T(4,128)}) fusion(f32[64,4,4,64]{3,2,1,0:T(4,128)S(1)} %mul.94, bf16[64,4,4,64]{3,1,2,0:T(4,128)(2,1)} %copy.142, bf16[64,4,4,64]{3,1,2,0:T(4,128)(2,1)S(1)} %copy.141, f32[64,4,4]{1,2,0:T(4,128)} %copy.140, f32[64,8,4]{1,2,0:T(4,128)} %copy-done.12, f32[64,8,4]{1,2,0:T(4,128)S(1)} %copy.136, ...), kind=kOutput, calls=%fused_computation.111 | convolution fusion | flops 6863872 | bytes 585760 | tf_op jit(solution)/shard_map/sthk,suhk->stuh/dot_general | solution.py:28
  97.8 1.8 %fusion.80 = f32[64,4,1,4]{3,2,1,0:T(1,128)S(1)} fusion(f32[64,4,64,1]{2,3,1,0:T(1,128)S(1)} %bitcast.149, f32[64,4,4,64]{3,2,1,0:T(4,128)S(1)} %mul.94), kind=kOutput, calls=%fused_computation.51 | convolution fusion | flops 786432 | bytes 331776 | tf_op jit(solution)/shard_map/shk,sthk->sth/dot_general | solution.py:35
  100.4 15.7 %fusion.78 = f32[64,4,4,64]{3,2,1,0:T(4,128)S(1)} fusion(f32[64,4,64,64]{3,2,1,0:T(8,128)} %param.30, f32[64,4,4,64]{3,2,1,0:T(4,128)S(1)} %mul.94), kind=kOutput, calls=%fused_computation.49 | convolution fusion | flops 50331648 | bytes 4718592 | tf_op jit(solution)/shard_map/shvk,sthk->sthv/dot_general | solution.py:32
  116.2 1.2 fusion.67
  118.1 2.5 %psum.7 = f32[64,4,4]{0,2,1:T(4,128)S(1)} all-reduce(f32[64,4,4]{0,2,1:T(4,128)S(1)} %multiply_reduce_fusion), channel_id=1, replica_groups=mesh['grp'=2,'dp'=2,'kv'=4,'tp'=2] {'tp'}, use_global_device_ids=true, to_apply=%region_5.6 | all-reduce | flops 1024 | bytes 8192 | tf_op jit(solution)/shard_map/psum | solution.py:134
  120.6 3.1 %fusion.134 = bf16[64,4,4096,1]{2,1,0,3:T(4,128)(2,1)S(1)} fusion(f32[4096]{0:T(1024)S(1)} %copy-done.23, f32[64,4]{1,0:T(8,128)S(1)} %copy-done.14, bf16[64,4,4096]{2,1,0:T(4,128)(2,1)} %all-gather.3.cloned.1.call-done), kind=kLoop, calls=%fused_computation.113 | loop fusion | flops 4194304 | bytes 4211712 | tf_op jit(solution)/shard_map/convert_element_type | solution.py:106
  123.8 2.1 %fusion.56 = bf16[64,4,4,64]{3,0,2,1:T(8,128)(2,1)S(1)} fusion(bf16[4096,4,64]{0,2,1:T(8,128)(2,1)S(1)} %copy-done.39, bf16[64,4,4096,1]{2,1,0,3:T(4,128)(2,1)S(1)} %fusion.134, f32[4,64]{1,0:T(4,128)S(1)} %copy-done.36, f32[64,4,4]{0,2,1:T(4,128)S(1)} %add_rsqrt_fusion.1, f32[64,4,4]{0,2,1:T(4,128)S(1)} %get-tuple-element.10, ...), kind=kOutput, calls=%fused_computation.31 | convolution fusion | flops 537526272 | bytes 4862976 | tf_op jit(solution)/shard_map/dot_general | solution.py:110
  126.2 0.9 reshape_reshape.3
  127.4 1.0 fusion.120
  129.5 12.3 %multiply_add_fusion = f32[64,4,64,64]{3,2,1,0:T(8,128)} fusion(f32[64,4,64,64]{3,2,1,0:T(8,128)} %param.30, f32[64,4]{1,0:T(8,128)S(1)} %copy.149, bf16[64,4,4,64]{3,1,2,0:T(4,128)(2,1)S(1)} %copy.141, f32[64,4,4,64]{3,2,1,0:T(4,128)S(1)} %convert_multiply_fusion.2), kind=kOutput, calls=%fused_computation | convolution fusion | flops 52428800 | bytes 8782848 | tf_op jit(solution)/shard_map/sjh,sjhv,sjhk->shvk/dot_general | solution.py:44
  141.8 7.4 %all-gather.5.cloned.1.call-done = bf16[8,256,256]{2,1,0:T(8,128)(2,1)} async-done(((bf16[1,256,256]{2,1,0:T(8,128)(2,1)}), bf16[8,256,256]{2,1,0:T(8,128)(2,1)}) %all-gather.5.cloned.1.call-update) | async-done | bytes 1048592 | tf_op jit(solution)/shard_map/all_gather | solution.py:144
  149.3 2.6 %fusion.31 = bf16[256,512]{1,0:T(8,128)(2,1)S(1)} fusion(bf16[8,256,256]{2,1,0:T(8,128)(2,1)} %all-gather.5.cloned.1.call-done, bf16[8,1,256,512]{3,2,1,0:T(8,128)(2,1)} %all-to-all-done), kind=kOutput, calls=%fused_computation.21 | convolution fusion | flops 537001984 | bytes 3407872 | tf_op jit(solution)/shard_map/gtc,gcd->td/dot_general | solution.py:142
  (123 shorter events, 13.7 us)
Async XLA Ops:
  7.2 73.0 %copy-start = (bf16[4096,4,64]{0,2,1:T(8,128)(2,1)S(1)}, bf16[4096,4,64]{0,2,1:T(8,128)(2,1)}, u32[]{:S(2)}) copy-start(bf16[4096,4,64]{0,2,1:T(8,128)(2,1)} %param.21) | copy-start | bytes 6291460
  7.2 51.6 %all-gather.3.cloned.1.call-start = ((), (), s32[]{:S(2)}) async-start(), calls=%async_computation.1 | async-start | bytes 2359296 | tf_op jit(solution)/shard_map/all_gather | solution.py:103
  7.9 6.9 %copy-start.3 = (bf16[4,64,4096]{2,1,0:T(8,128)(2,1)S(1)}, bf16[4,64,4096]{2,1,0:T(8,128)(2,1)}, u32[]{:S(2)}) copy-start(bf16[4,64,4096]{2,1,0:T(8,128)(2,1)} %param.29) | copy-start | bytes 6291460
  17.7 6.6 %copy-start.15 = (bf16[64,4,4,64]{3,2,1,0:T(4,128)(2,1)S(1)}, bf16[64,4,4,64]{3,2,1,0:T(4,128)(2,1)}, u32[]{:S(2)}) copy-start(bf16[64,4,4,64]{3,2,1,0:T(4,128)(2,1)} %param.33) | copy-start | bytes 393220
  17.7 6.7 %copy-start.4 = (bf16[64,4,4,64]{3,2,1,0:T(4,128)(2,1)S(1)}, bf16[64,4,4,64]{3,2,1,0:T(4,128)(2,1)}, u32[]{:S(2)}) copy-start(bf16[64,4,4,64]{3,2,1,0:T(4,128)(2,1)} %param.34) | copy-start | bytes 393220
  17.7 7.5 %copy-start.40 = (f32[16]{0:T(128)S(1)}, f32[16]{0:T(128)}, u32[]{:S(2)}) copy-start(f32[16]{0:T(128)} %param.27) | copy-start | bytes 196
  17.7 9.0 %copy-start.38 = (s32[64]{0:T(128)S(1)}, s32[64]{0:T(128)}, u32[]{:S(2)}) copy-start(s32[64]{0:T(128)} %param.37) | copy-start | bytes 772
  17.7 124.1 %all-to-all-start = ((bf16[8,1,256,512]{3,2,1,0:T(8,128)(2,1)}), bf16[8,1,256,512]{3,2,1,0:T(8,128)(2,1)}, u32[]{:S(2)}, u32[]{:S(2)}) async-start(bf16[8,1,256,512]{3,2,1,0:T(8,128)(2,1)} %fusion.83), calls=%async_computation | async-start | bytes 4194304 | tf_op jit(solution)/shard_map/all_to_all | solution.py:81
  24.2 37.5 %copy-start.22 = (f32[4096]{0:T(1024)S(1)}, f32[4096]{0:T(1024)}, u32[]{:S(2)}) copy-start(f32[4096]{0:T(1024)} %param.20) | copy-start | bytes 49156
  24.2 125.0 %all-gather.5.cloned.1.call-start = ((), (), s32[]{:S(2)}) async-start(), calls=%async_computation.2 | async-start | bytes 1179648 | tf_op jit(solution)/shard_map/all_gather | solution.py:144
  26.8 51.2 %copy-start.37 = (pred[4,8]{1,0:T(4,128)(4,1)}, pred[4,8]{1,0:T(4,128)(4,1)S(1)}, u32[]{:S(2)}) copy-start(pred[4,8]{1,0:T(4,128)(4,1)S(1)} %iota_compare_fusion.1) | copy-start | bytes 100
  68.9 9.9 %copy-start.28 = (f32[64,4]{0,1:T(4,128)}, f32[64,4]{0,1:T(4,128)S(1)}, u32[]{:S(2)}) copy-start(f32[64,4]{0,1:T(4,128)S(1)} %slice_bitcast_fusion.8) | copy-start | bytes 3076
  73.1 4.7 %copy-start.33 = (f32[64,4,4]{0,2,1:T(4,128)S(1)}, f32[64,4,4]{0,2,1:T(4,128)}, u32[]{:S(2)}) copy-start(f32[64,4,4]{0,2,1:T(4,128)} %param.35) | copy-start | bytes 12292
  73.1 5.7 %copy-start.26 = (f32[64,4]{0,1:T(4,128)S(1)}, f32[64,4]{0,1:T(4,128)}, u32[]{:S(2)}) copy-start(f32[64,4]{0,1:T(4,128)} %param.32) | copy-start | bytes 3076
  73.2 7.0 %copy-start.11 = (f32[64,4,4]{1,2,0:T(4,128)}, f32[64,4,4]{1,2,0:T(4,128)S(1)}, u32[]{:S(2)}) copy-start(f32[64,4,4]{1,2,0:T(4,128)S(1)} %copy.135) | copy-start | bytes 12292
  85.9 4.4 %copy-start.6 = (bf16[64,4,4,64]{3,2,1,0:T(4,128)(2,1)}, bf16[64,4,4,64]{3,2,1,0:T(4,128)(2,1)S(1)}, u32[]{:S(2)}) copy-start(bf16[64,4,4,64]{3,2,1,0:T(4,128)(2,1)S(1)} %reshape.166) | copy-start | bytes 393220
  91.5 5.6 %copy-start.7 = (bf16[64,4,4,64]{3,2,1,0:T(4,128)(2,1)}, bf16[64,4,4,64]{3,2,1,0:T(4,128)(2,1)S(1)}, u32[]{:S(2)}) copy-start(bf16[64,4,4,64]{3,2,1,0:T(4,128)(2,1)S(1)} %reshape.164) | copy-start | bytes 393220
  93.6 4.2 %copy-start.18 = (f32[64,4,64]{2,1,0:T(4,128)S(1)}, f32[64,4,64]{2,1,0:T(4,128)}, u32[]{:S(2)}) copy-start(f32[64,4,64]{2,1,0:T(4,128)} %param.31) | copy-start | bytes 196612
  100.3 15.8 %copy-start.8 = (bf16[64,4,4,64]{3,1,2,0:T(4,128)(2,1)S(1)}, bf16[64,4,4,64]{3,1,2,0:T(4,128)(2,1)}, u32[]{:S(2)}) copy-start(bf16[64,4,4,64]{3,1,2,0:T(4,128)(2,1)} %copy.132) | copy-start | bytes 393220
  100.3 15.8 %copy-start.9 = (bf16[64,4,4,64]{3,1,2,0:T(4,128)(2,1)S(1)}, bf16[64,4,4,64]{3,1,2,0:T(4,128)(2,1)}, u32[]{:S(2)}) copy-start(bf16[64,4,4,64]{3,1,2,0:T(4,128)(2,1)} %copy.133) | copy-start | bytes 393220
  100.3 15.8 %copy-start.10 = (f32[64,4,8,4]{2,1,3,0:T(4,128)S(1)}, f32[64,4,8,4]{2,1,3,0:T(4,128)}, u32[]{:S(2)}) copy-start(f32[64,4,8,4]{2,1,3,0:T(4,128)} %get-tuple-element.16) | copy-start | bytes 98308
  100.3 17.0 %copy-start.17 = (f32[64,8,4]{0,2,1:T(4,128)S(1)}, f32[64,8,4]{0,2,1:T(4,128)}, u32[]{:S(2)}) copy-start(f32[64,8,4]{0,2,1:T(4,128)} %copy-done.16) | copy-start | bytes 24580
  100.4 17.0 %copy-start.21 = (f32[64,4,4]{0,2,1:T(4,128)S(1)}, f32[64,4,4]{0,2,1:T(4,128)}, u32[]{:S(2)}) copy-start(f32[64,4,4]{0,2,1:T(4,128)} %copy-done.20) | copy-start | bytes 12292
  100.4 17.0 %copy-start.24 = (f32[64,4,4]{0,2,1:T(4,128)S(1)}, f32[64,4,4]{0,2,1:T(4,128)}, u32[]{:S(2)}) copy-start(f32[64,4,4]{0,2,1:T(4,128)} %copy.147) | copy-start | bytes 12292
  100.4 17.0 %copy-start.25 = (f32[64,4,1,4]{0,1,3,2:T(4,128)S(1)}, f32[64,4,1,4]{0,1,3,2:T(4,128)}, u32[]{:S(2)}) copy-start(f32[64,4,1,4]{0,1,3,2:T(4,128)} %copy.156) | copy-start | bytes 12292
  100.4 17.0 %copy-start.27 = (f32[64,4]{0,1:T(4,128)S(1)}, f32[64,4]{0,1:T(4,128)}, u32[]{:S(2)}) copy-start(f32[64,4]{0,1:T(4,128)} %param.32) | copy-start | bytes 3076
  100.4 17.0 %copy-start.29 = (f32[64,4]{0,1:T(4,128)S(1)}, f32[64,4]{0,1:T(4,128)}, u32[]{:S(2)}) copy-start(f32[64,4]{0,1:T(4,128)} %copy-done.28) | copy-start | bytes 3076
  100.4 17.0 %copy-start.30 = (f32[64,4]{0,1:T(4,128)S(1)}, f32[64,4]{0,1:T(4,128)}, u32[]{:S(2)}) copy-start(f32[64,4]{0,1:T(4,128)} %get-tuple-element.9) | copy-start | bytes 3076
  116.1 4.4 %copy-start.14 = (f32[64,4]{1,0:T(8,128)S(1)}, f32[64,4]{1,0:T(8,128)}, u32[]{:S(2)}) copy-start(f32[64,4]{1,0:T(8,128)} %copy-done.13) | copy-start | bytes 3076
  116.1 4.5 %copy-start.23 = (f32[4096]{0:T(1024)S(1)}, f32[4096]{0:T(1024)}, u32[]{:S(2)}) copy-start(f32[4096]{0:T(1024)} %param.20) | copy-start | bytes 49156
  123.8 3.4 %copy-start.31 = (f32[64,4]{0,1:T(4,128)S(1)}, f32[64,4]{0,1:T(4,128)}, u32[]{:S(2)}) copy-start(f32[64,4]{0,1:T(4,128)} %get-tuple-element.8) | copy-start | bytes 3076
  125.9 3.3 %copy-start.5 = (bf16[64,4,4,64]{3,2,1,0:T(4,128)(2,1)S(1)}, bf16[64,4,4,64]{3,2,1,0:T(4,128)(2,1)}, u32[]{:S(2)}) copy-start(bf16[64,4,4,64]{3,2,1,0:T(4,128)(2,1)} %param.34) | copy-start | bytes 393220
  (12 other events, 24.9 us)
Sparse Core Ops, SparseCore 0:
  9.6 49.1 all-gather.2
  127.2 22.0 all-gather.4
